TPU v7x, 32 devices: a whole 2x2x4 slice. The times are simulated.
32 devices in a mesh: sp: 4 (over z), fs: 4 (over y, x), tp: 2 (over core).
Axes of the slice: x: 2, y: 2, z: 4, core: 2. Of those that a mesh axis runs over, the one named last changes fastest.
Arguments:
- tokens: bfloat16 [4096, 2048], P(('fs', 'sp')), parts along dimension 0, may hold values from -6 to 6
- norm_gain: float32 [2048], replicated, may hold values from 0.1 to 1.9
- w_query: bfloat16 [2048, 1024], P('sp', 'tp'), may hold values from -0.080939698 to 0.080939698
- w_key: bfloat16 [2048, 256], P('sp', 'tp'), may hold values from -0.080939698 to 0.080939698
- w_value: bfloat16 [2048, 256], P('sp', 'tp'), may hold values from -0.125 to 0.125
- w_conv_in: bfloat16 [2048, 1024], P('sp', 'tp'), may hold values from -0.125 to 0.125
- w_conv_gate: bfloat16 [2048, 1024], P('sp', 'tp'), may hold values from -0.125 to 0.125
- sink_logit: float32 [16], P('tp'), may hold values from 2 to 6
- conv_taps: float32 [31, 1024], P(None, 'tp'), may hold values from -5.3881591 to 5.3881591
- conv_bias: float32 [1024], P('tp'), may hold values from -0.9 to 5.9
- channel_gain: float32 [1024], P('tp'), may hold values from 0.1 to 1.9
- channel_shift: float32 [1024], P('tp'), may hold values from -3 to 3
- w_attn_out: bfloat16 [1024, 2048], P(None, 'sp'), may hold values from -1.5 to 1.5
- w_conv_out: bfloat16 [1024, 2048], P(None, 'sp'), may hold values from -0.1875 to 0.1875
Outputs:
- output: bfloat16 [4096, 2048], P(('fs', 'sp', 'tp')), parts along dimension 0
There are 4 independent parts, one for each index of `fs`. A program takes and returns all parts, laid end to end along the dimension named above; an argument that names none is the same for every part. Nothing has to cross between parts.
All inputs are finite; a program needn't handle non-finite values.
Results may differ from a plain program's by a relative error of at most 0.011.
Values may be sent and summed in bfloat16 or wider, within the bound.
A program may use at most 64 MiB of HBM per device.

v0:
```python
import jax
import jax.numpy as jnp
from jax import lax
from jax.sharding import PartitionSpec as P

HEAD_DIM = 64
WINDOW = 128
GRID_W = 64
EPSILON = 1e-06
NEGATIVE = -1e30
ROPE_BASE = 10000.0


def padded(block, sides, width):
    for axis, dim in sides:
        count = lax.axis_size(axis)
        forward = [(i, i + 1) for i in range(count - 1)]
        backward = [(target, source) for source, target in forward]
        low = lax.ppermute(
            lax.slice_in_dim(block, block.shape[dim] - width, None, axis=dim), axis, forward
        )
        high = lax.ppermute(lax.slice_in_dim(block, 0, width, axis=dim), axis, backward)
        block = jnp.concatenate([low, block, high], axis=dim)
    return block


def rotate_pairs(values, positions):
    middle = values.shape[-1] // 2
    inverse = ROPE_BASE ** (-jnp.arange(middle, dtype=jnp.float32) / middle)
    angles = positions.astype(jnp.float32)[:, None] * inverse[None, :]
    cosine = jnp.cos(angles)[:, None, :]
    sine_table = jnp.sin(angles)[:, None, :]
    leading = values[..., :middle]
    trailing = values[..., middle:]
    return jnp.concatenate(
        [leading * cosine - trailing * sine_table, leading * sine_table + trailing * cosine],
        axis=-1,
    )


def grid_rotate(values, positions):
    middle = values.shape[-1] // 2
    return jnp.concatenate(
        [
            rotate_pairs(values[..., :middle], positions // GRID_W),
            rotate_pairs(values[..., middle:], positions % GRID_W),
        ],
        axis=-1,
    )


def local(
    tokens,
    norm_gain,
    w_query,
    w_key,
    w_value,
    w_conv_in,
    w_conv_gate,
    sink_logit,
    conv_taps,
    conv_bias,
    channel_gain,
    channel_shift,
    w_attn_out,
    w_conv_out,
):
    rows_here = tokens.shape[0]
    offset = lax.axis_index("sp") * rows_here
    total = rows_here * lax.axis_size("sp")
    tp_count = lax.axis_size("tp")
    token_float = tokens.astype(jnp.float32)
    normed = (
        token_float
        * lax.rsqrt(jnp.mean(token_float * token_float, axis=-1, keepdims=True) + EPSILON)
        * norm_gain[None, :]
    ).astype(jnp.bfloat16)
    head_cols = w_query.shape[1]
    kv_cols = w_key.shape[1]
    chan_cols = w_conv_in.shape[1]
    piece_query = lax.all_gather(w_query, "sp", axis=0, tiled=True)
    piece_key = lax.all_gather(w_key, "sp", axis=0, tiled=True)
    piece_value = lax.all_gather(w_value, "sp", axis=0, tiled=True)
    piece_conv = lax.all_gather(w_conv_in, "sp", axis=0, tiled=True)
    piece_gate = lax.all_gather(w_conv_gate, "sp", axis=0, tiled=True)
    query_acc = jnp.dot(normed, piece_query, preferred_element_type=jnp.float32)
    pair_acc = jnp.dot(
        normed,
        jnp.concatenate([piece_key, piece_value], axis=1),
        preferred_element_type=jnp.float32,
    )
    conv_acc = jnp.dot(
        normed,
        jnp.concatenate([piece_conv, piece_gate], axis=1),
        preferred_element_type=jnp.float32,
    )
    positions = offset + jnp.arange(rows_here, dtype=jnp.int32)
    heads_here = head_cols // HEAD_DIM
    kv_here = kv_cols // HEAD_DIM
    group = heads_here // kv_here
    query = grid_rotate(query_acc.reshape(rows_here, heads_here, HEAD_DIM), positions).astype(
        jnp.bfloat16
    )
    keys = grid_rotate(pair_acc[:, :kv_cols].reshape(rows_here, kv_here, HEAD_DIM), positions)
    keys = keys.astype(jnp.bfloat16).reshape(rows_here, kv_cols)
    values = pair_acc[:, kv_cols:].astype(jnp.bfloat16)
    stacked = jnp.concatenate([keys, values], axis=1)
    extended = padded(stacked, (("sp", 0),), WINDOW)
    block = min(rows_here, 512)
    span = block + 2 * WINDOW
    sinks = sink_logit.reshape(kv_here, group)[:, :, None, None]
    queries = query.reshape(block, kv_here, group, HEAD_DIM)
    near_keys = extended[:, :kv_cols].reshape(span, kv_here, HEAD_DIM)
    near_values = extended[:, kv_cols:].reshape(span, kv_here, HEAD_DIM)
    scores = jnp.einsum(
        "qkgd,skd->kgqs", queries, near_keys, preferred_element_type=jnp.float32
    ) * HEAD_DIM ** (-0.5)
    query_pos = offset + 0 + jnp.arange(block, dtype=jnp.int32)
    key_pos = offset + 0 - WINDOW + jnp.arange(span, dtype=jnp.int32)
    valid = (
        (jnp.abs(query_pos[:, None] - key_pos[None, :]) <= WINDOW)
        & (key_pos[None, :] >= 0)
        & (key_pos[None, :] < total)
    )
    scores = jnp.where(valid[None, None], scores, NEGATIVE)
    top = jnp.maximum(jnp.max(scores, axis=-1, keepdims=True), sinks)
    raised = jnp.exp(scores - top)
    denominator = jnp.sum(raised, axis=-1, keepdims=True) + jnp.exp(sinks - top)
    probs = (raised / denominator).astype(jnp.bfloat16)
    mixed = jnp.einsum("kgqs,skd->qkgd", probs, near_values, preferred_element_type=jnp.float32)
    outputs = mixed.astype(jnp.bfloat16).reshape(block, head_cols)
    glu = (conv_acc[:, :chan_cols] * jax.nn.sigmoid(conv_acc[:, chan_cols:])).astype(jnp.bfloat16)
    reach = conv_taps.shape[0] // 2
    rims = padded(glu, (("sp", 0),), reach)
    filtered = jnp.zeros((rows_here, chan_cols), jnp.float32) + conv_bias[None, :]
    for shift_index in range(conv_taps.shape[0]):
        filtered = filtered + conv_taps[shift_index][None, :] * rims[
            shift_index : shift_index + rows_here
        ].astype(jnp.float32)
    channel_total = chan_cols * tp_count
    centre = lax.psum(jnp.sum(filtered, axis=-1), "tp")[:, None] / channel_total
    centred = filtered - centre
    spread = lax.psum(jnp.sum(centred * centred, axis=-1), "tp")[:, None] / channel_total
    conv_out = jax.nn.silu(
        centred * lax.rsqrt(spread + EPSILON) * channel_gain[None, :] + channel_shift[None, :]
    ).astype(jnp.bfloat16)
    features = jnp.concatenate([outputs, conv_out], axis=1)
    tp_here = lax.axis_index("tp")
    own_rows = jnp.concatenate(
        [
            lax.dynamic_slice_in_dim(w_attn_out, tp_here * head_cols, head_cols, 0),
            lax.dynamic_slice_in_dim(w_conv_out, tp_here * chan_cols, chan_cols, 0),
        ],
        axis=0,
    )
    own_whole = lax.all_gather(own_rows, "sp", axis=1, tiled=True)
    result = lax.psum_scatter(
        jnp.dot(features, own_whole, preferred_element_type=jnp.float32).astype(jnp.bfloat16),
        "tp",
        scatter_dimension=0,
        tiled=True,
    )
    return result


def solution(mesh):
    in_specs = (
        P(("fs", "sp"), None),
        P(),
        P("sp", "tp"),
        P("sp", "tp"),
        P("sp", "tp"),
        P("sp", "tp"),
        P("sp", "tp"),
        P("tp"),
        P(None, "tp"),
        P("tp"),
        P("tp"),
        P("tp"),
        P(None, "sp"),
        P(None, "sp"),
    )
    out_specs = P(("fs", "sp", "tp"), None)
    return jax.shard_map(local, mesh=mesh, in_specs=in_specs, out_specs=out_specs, check_vma=False)
```

profile of v0, /device:TPU:0, one launch (start us, length us, event | category | flops | bytes accessed | tf_op | source)
XLA Modules:
  0.0 263.5 jit_solution(13735289390232705822)
XLA Ops:
  6.5 0.7 all-gather.7.cloned.1.call-update
  7.3 0.0 all-gather.9.cloned.1.call-start
  7.3 0.7 all-gather.9.cloned.1.call-update
  8.0 0.0 all-gather.5.cloned.1.call-start
  8.1 0.7 all-gather.5.cloned.1.call-update
  8.8 0.0 all-gather.11.cloned.1.call-start
  8.8 1.3 constant_dynamic-slice_fusion
  10.1 1.0 pad_maximum_fusion
  11.1 0.0 all-gather.11.cloned.1.call-update
  11.2 0.0 reduce-scatter.2.cloned.1.call-start
  11.3 0.3 fusion.6
  11.6 23.1 %all_gather.18 = bf16[2048,128]{1,0:T(8,128)(2,1)S(1)} all-gather(bf16[512,128]{1,0:T(8,128)(2,1)S(1)} %copy-done.1), channel_id=1, replica_groups=mesh['sp'=4,'fs'=4,'tp'=2] {'sp'}, dimensions={0}, use_global_device_ids=true | all-gather | bytes 655360 | tf_op jit(solution)/shard_map/all_gather | solution.py:82
  34.7 21.7 %all_gather.19 = bf16[2048,128]{1,0:T(8,128)(2,1)S(1)} all-gather(bf16[512,128]{1,0:T(8,128)(2,1)S(1)} %copy-done.2), channel_id=1, replica_groups=mesh['sp'=4,'fs'=4,'tp'=2] {'sp'}, dimensions={0}, use_global_device_ids=true | all-gather | bytes 655360 | tf_op jit(solution)/shard_map/all_gather | solution.py:83
  56.4 0.7 fusion.11
  57.1 0.2 multiply_cosine_fusion.1
  57.4 1.5 collective-permute-start
  58.9 1.3 collective-permute-start.1
  60.3 0.3 fusion.24
  60.6 0.1 max.18
  60.7 1.5 collective-permute-done
  62.2 7.0 %collective-permute-done.1 = bf16[128,256]{0,1:T(8,128)(2,1)S(1)} collective-permute-done((bf16[128,256]{0,1:T(8,128)(2,1)S(1)}, bf16[128,256]{0,1:T(8,128)(2,1)S(1)}, u32[]{:S(2)}, u32[]{:S(2)}) %collective-permute-start.1) | collective-permute-done | bytes 65568 | tf_op jit(solution)/shard_map/ppermute | solution.py:22
  69.2 1.9 all-gather.7.cloned.1.call-done
  71.1 47.3 %all-gather.9.cloned.1.call-done = bf16[2048,512]{1,0:T(8,128)(2,1)} async-done(((bf16[512,512]{1,0:T(8,128)(2,1)}), bf16[2048,512]{1,0:T(8,128)(2,1)}) %all-gather.9.cloned.1.call-update) | async-done | bytes 2097168 | tf_op jit(solution)/shard_map/all_gather | solution.py:85
  118.4 3.5 %fusion = f32[256,1024]{1,0:T(8,128)S(1)} fusion(bf16[2048,512]{1,0:T(8,128)(2,1)} %all-gather.9.cloned.1.call-done, bf16[2048,512]{1,0:T(8,128)(2,1)} %all-gather.7.cloned.1.call-done, bf16[256,2048]{1,0:T(8,128)(2,1)S(1)} %copy-done, f32[2048]{0:T(1024)S(1)} %copy-done.7, f32[256]{0:T(256)S(1)} %add_rsqrt_fusion.1), kind=kOutput, calls=%fused_computation | convolution fusion | flops 1084227584 | bytes 6300672 | tf_op jit(solution)/shard_map/dot_general | solution.py:92
  121.9 0.1 fusion.22
  122.1 2.1 collective-permute-start.2
  124.2 1.3 collective-permute-start.3
  125.5 39.2 %all-gather.5.cloned.1.call-done = bf16[2048,512]{1,0:T(8,128)(2,1)} async-done(((bf16[512,512]{1,0:T(8,128)(2,1)}), bf16[2048,512]{1,0:T(8,128)(2,1)}) %all-gather.5.cloned.1.call-update) | async-done | bytes 2097168 | tf_op jit(solution)/shard_map/all_gather | solution.py:81
  164.6 2.6 fusion.74
  167.2 0.1 subtract_convert_fusion.1
  167.3 0.8 fusion.5
  168.2 0.1 broadcast_maximum_fusion
  168.2 0.9 fusion.4
  169.1 0.1 exponential_add_fusion
  169.2 0.0 copy-start.4
  169.2 0.0 copy-start.5
  169.2 0.0 copy-start.6
  169.3 1.2 fusion.10
  170.5 0.1 copy.27
  170.7 3.1 %fusion.77 = (f32[256]{0:T(256)S(1)}, f32[256,512]{1,0:T(8,128)S(1)}) fusion(bf16[15,512]{1,0:T(8,128)(2,1)S(1)} %collective-permute-done.3, bf16[256,512]{1,0:T(8,128)(2,1)S(1)} %fusion.22, f32[512]{0:T(512)S(1)} %bitcast.106, f32[512]{0:T(512)S(1)} %bitcast.107, f32[512]{0:T(512)S(1)} %bitcast.78, f32[512]{0:T(512)S(1)} %bitcast.79, f32[512]{0:T(512)S(1)} %bitcast.80, ...), kind=kLoop, calls=%fused_computation.167 | loop fusion | flops 24116992 | bytes 883712 | tf_op jit(solution)/shard_map/reduce_sum | solution.py:141
  173.8 2.5 psum.14
  176.2 0.2 multiply_reduce_fusion
  176.4 2.5 psum.15
  178.9 0.3 multiply_convert_fusion
  179.2 66.3 %all-gather.11.cloned.1.call-done = bf16[1024,2048]{1,0:T(8,128)(2,1)} async-done(((bf16[1024,512]{1,0:T(8,128)(2,1)}), bf16[1024,2048]{1,0:T(8,128)(2,1)}) %all-gather.11.cloned.1.call-update) | async-done | bytes 4194320 | tf_op jit(solution)/shard_map/all_gather | solution.py:156
  245.5 4.5 %convolution_convert_fusion = bf16[256,2048]{1,0:T(8,128)(2,1)} fusion(bf16[1024,2048]{1,0:T(8,128)(2,1)} %all-gather.11.cloned.1.call-done, bf16[256,512]{1,0:T(8,128)(2,1)S(1)} %multiply_convert_fusion, bf16[256,512]{1,0:T(8,128)(2,1)S(1)} %copy.27), kind=kOutput, calls=%fused_computation.11 | convolution fusion | flops 1075314688 | bytes 5767168 | tf_op jit(solution)/shard_map/dot_general | solution.py:158
  249.9 0.0 reduce-scatter.2.cloned.1.call-update
  249.9 7.0 %reduce-scatter.2.cloned.1.call-done = bf16[128,2048]{1,0:T(8,128)(2,1)} async-done(((bf16[256,2048]{1,0:T(8,128)(2,1)}), bf16[128,2048]{1,0:T(8,128)(2,1)}) %reduce-scatter.2.cloned.1.call-update) | async-done | bytes 524304 | tf_op jit(solution)/shard_map/reduce_scatter | solution.py:157
  (36 shorter events, 0.3 us)
Async XLA Ops:
  6.5 4.7 %copy-start = (bf16[256,2048]{1,0:T(8,128)(2,1)S(1)}, bf16[256,2048]{1,0:T(8,128)(2,1)}, u32[]{:S(2)}) copy-start(bf16[256,2048]{1,0:T(8,128)(2,1)} %param.14) | copy-start | bytes 3145732
  6.5 5.0 %copy-start.1 = (bf16[512,128]{1,0:T(8,128)(2,1)S(1)}, bf16[512,128]{1,0:T(8,128)(2,1)}, u32[]{:S(2)}) copy-start(bf16[512,128]{1,0:T(8,128)(2,1)} %param.17) | copy-start | bytes 393220
  6.5 28.1 %copy-start.2 = (bf16[512,128]{1,0:T(8,128)(2,1)S(1)}, bf16[512,128]{1,0:T(8,128)(2,1)}, u32[]{:S(2)}) copy-start(bf16[512,128]{1,0:T(8,128)(2,1)} %param.18) | copy-start | bytes 393220
  6.5 64.6 %all-gather.7.cloned.1.call-start = ((), (), s32[]{:S(2)}) async-start(), calls=%async_computation.2 | async-start | bytes 2621440 | tf_op jit(solution)/shard_map/all_gather | solution.py:84
  7.3 111.1 %all-gather.9.cloned.1.call-start = ((), (), s32[]{:S(2)}) async-start(), calls=%async_computation.3 | async-start | bytes 2621440 | tf_op jit(solution)/shard_map/all_gather | solution.py:85
  8.0 48.4 %copy-start.7 = (f32[2048]{0:T(1024)S(1)}, f32[2048]{0:T(1024)}, u32[]{:S(2)}) copy-start(f32[2048]{0:T(1024)} %param.15) | copy-start | bytes 24580
  8.0 156.6 %all-gather.5.cloned.1.call-start = ((), (), s32[]{:S(2)}) async-start(), calls=%async_computation.1 | async-start | bytes 2621440 | tf_op jit(solution)/shard_map/all_gather | solution.py:81
  8.8 236.7 %all-gather.11.cloned.1.call-start = ((), (), s32[]{:S(2)}) async-start(), calls=%async_computation.4 | async-start | bytes 5242880 | tf_op jit(solution)/shard_map/all_gather | solution.py:156
  11.1 49.1 %copy-start.3 = (f32[31,512]{1,0:T(8,128)S(1)}, f32[31,512]{1,0:T(8,128)}, u32[]{:S(2)}) copy-start(f32[31,512]{1,0:T(8,128)} %param.22) | copy-start | bytes 190468
  11.1 49.5 %copy-start.8 = (f32[8]{0:T(128)S(1)}, f32[8]{0:T(128)}, u32[]{:S(2)}) copy-start(f32[8]{0:T(128)} %param.21) | copy-start | bytes 100
  11.2 245.8 %reduce-scatter.2.cloned.1.call-start = ((), (), s32[]{:S(2)}) async-start(), calls=%async_computation.5 | async-start | bytes 1572864 | tf_op jit(solution)/shard_map/reduce_scatter | solution.py:157
  57.4 4.8 %collective-permute-start = (bf16[128,256]{0,1:T(8,128)(2,1)S(1)}, bf16[128,256]{0,1:T(8,128)(2,1)S(1)}, u32[]{:S(2)}, u32[]{:S(2)}) collective-permute-start(bf16[128,256]{0,1:T(8,128)(2,1)S(1)} %get-tuple-element.21), channel_id=1, source_target_pairs={{0,8},{8,16},{16,24},{1,9},{9,17},{17,25},{2,10},{10,18},{18,26},{... | collective-permute-start | bytes 196616 | tf_op jit(solution)/shard_map/ppermute | solution.py:19
  58.9 10.3 %collective-permute-start.1 = (bf16[128,256]{0,1:T(8,128)(2,1)S(1)}, bf16[128,256]{0,1:T(8,128)(2,1)S(1)}, u32[]{:S(2)}, u32[]{:S(2)}) collective-permute-start(bf16[128,256]{0,1:T(8,128)(2,1)S(1)} %get-tuple-element.22), channel_id=1, source_target_pairs={{8,0},{16,8},{24,16},{9,1},{17,9},{25,17},{10,2},{18,10},{26,18},{... | collective-permute-start | bytes 196616 | tf_op jit(solution)/shard_map/ppermute | solution.py:22
  122.1 48.6 %collective-permute-start.2 = (bf16[15,512]{1,0:T(8,128)(2,1)S(1)}, bf16[15,512]{1,0:T(8,128)(2,1)S(1)}, u32[]{:S(2)}, u32[]{:S(2)}) collective-permute-start(bf16[15,512]{1,0:T(8,128)(2,1)S(1)} %get-tuple-element.15), channel_id=1, source_target_pairs={{0,8},{8,16},{16,24},{1,9},{9,17},{17,25},{2,10},{10,18},{18,26},{... | collective-permute-start | bytes 46088 | tf_op jit(solution)/shard_map/ppermute | solution.py:19
  124.2 46.5 %collective-permute-start.3 = (bf16[15,512]{1,0:T(8,128)(2,1)S(1)}, bf16[15,512]{1,0:T(8,128)(2,1)S(1)}, u32[]{:S(2)}, u32[]{:S(2)}) collective-permute-start(bf16[15,512]{1,0:T(8,128)(2,1)S(1)} %get-tuple-element.16), channel_id=1, source_target_pairs={{8,0},{16,8},{24,16},{9,1},{17,9},{25,17},{10,2},{18,10},{26,18},{... | collective-permute-start | bytes 46088 | tf_op jit(solution)/shard_map/ppermute | solution.py:22
  169.2 1.4 copy-start.4
  169.2 9.7 %copy-start.5 = (f32[512]{0:T(512)S(1)}, f32[512]{0:T(512)}, u32[]{:S(2)}) copy-start(f32[512]{0:T(512)} %param.25) | copy-start | bytes 6148
  169.2 9.7 %copy-start.6 = (f32[512]{0:T(512)S(1)}, f32[512]{0:T(512)}, u32[]{:S(2)}) copy-start(f32[512]{0:T(512)} %param.24) | copy-start | bytes 6148
Sparse Core Ops, SparseCore 0:
  8.9 62.1 all-gather.6
  72.7 45.6 all-gather.8
  120.0 44.6 all-gather.4
  166.1 79.3 all-gather.10
  250.1 6.8 reduce-scatter.1
where the time goes:
time: 264 us
  waiting for transfers between devices  172 us (65%)
  blocking collectives  49.7 us (19%)
  between operations  13.5 us (5%)
  matrix products  13.3 us (5%)
  other arithmetic  6.78 us (3%)
  starting transfers between devices  6.35 us (2%)
    all_gather x1, waiting for transfers between devices, local(): own_whole = lax.all_gather(own_rows, 'sp', axis=1, tiled=True)  66.3 us
    all_gather x1, waiting for transfers between devices, local(): piece_gate = lax.all_gather(w_conv_gate, 'sp', axis=0, tiled=True)  47.3 us
    all_gather x1, waiting for transfers between devices, local(): piece_query = lax.all_gather(w_query, 'sp', axis=0, tiled=True)  39.2 us
    all_gather x1, blocking collectives, local(): piece_key = lax.all_gather(w_key, 'sp', axis=0, tiled=True)  23.1 us
    all_gather x1, blocking collectives, local(): piece_value = lax.all_gather(w_value, 'sp', axis=0, tiled=True)  21.7 us
    reduce_scatter x1, waiting for transfers between devices, local(): lax.psum_scatter(jnp.dot(features, own_whole, preferred_element_type=jnp....  7.04 us
    ppermute x2, waiting for transfers between devices, padded(): lax.ppermute(lax.slice_in_dim(block, 0, width, axis=dim), axis, backward)  6.99 us
  transfers between devices with their start and end apart: 9, of which 7 were waited for; matrix products, arithmetic and copies ran while one was open for 7% of the time, Pallas kernels for 0%

commit v1 on v0

--- a/solution.py
+++ b/solution.py
@@ -78,7 +78,12 @@
     head_cols = w_query.shape[1]
     kv_cols = w_key.shape[1]
     chan_cols = w_conv_in.shape[1]
-    piece_query = lax.all_gather(w_query, "sp", axis=0, tiled=True)
+    ring = [w_query]
+    for hop in range(3):
+        ring.append(lax.ppermute(ring[-1], "sp", [(dev, (dev + 1) % 4) for dev in range(4)]))
+    piece_query = jnp.roll(
+        jnp.concatenate(ring[::-1], axis=0), (lax.axis_index("sp") + 1) * ring[0].shape[0], axis=0
+    )
     piece_key = lax.all_gather(w_key, "sp", axis=0, tiled=True)
     piece_value = lax.all_gather(w_value, "sp", axis=0, tiled=True)
     piece_conv = lax.all_gather(w_conv_in, "sp", axis=0, tiled=True)

time: 264 us -> 235 us (0.89)
  waiting for transfers between devices: 172 us -> 108 us
  starting transfers between devices: 6.35 us -> 21.7 us
  blocking collectives: 49.7 us -> 63 us
  local copies, waits for them, and re-layouts: 1.64 us -> 6.3 us
    all_gather x1, waiting for transfers between devices: 47.3 us -> 3.7 us  [local(): piece_gate = lax.all_gather(w_conv_gate, 'sp', axis=0, tiled=True)]
    all_gather x1 -> x0, waiting for transfers between devices: 39.2 us -> none  [local(): piece_query = lax.all_gather(w_query, 'sp', axis=0, tiled=True)]
    ppermute x0 -> x3, waiting for transfers between devices: none -> 36 us  [local(): lax.ppermute(ring[-1], 'sp', [(dev, (dev + 1) % 4) for dev in range(4)])]
    all_gather x1, blocking collectives: 23.1 us -> 37.8 us  [local(): piece_key = lax.all_gather(w_key, 'sp', axis=0, tiled=True)]
    all_gather x1, waiting for transfers between devices: 66.3 us -> 53.4 us  [local(): own_whole = lax.all_gather(own_rows, 'sp', axis=1, tiled=True)]
    ppermute x0 -> x3, starting transfers between devices: none -> 9.96 us  [local(): lax.ppermute(ring[-1], 'sp', [(dev, (dev + 1) % 4) for dev in range(4)])]
    ppermute x2, starting transfers between devices: 3.61 us -> 9.02 us  [padded(): lax.ppermute(lax.slice_in_dim(block, block.shape[dim] - width, None, axis...]
  transfers between devices with their start and end apart: 9 -> 11, of which waited for: 7 -> 6; matrix products, arithmetic and copies ran while one was open for 7% -> 9% of each run, Pallas kernels for 0% -> 0%
where the time goes in v1:
time: 235 us
  waiting for transfers between devices  108 us (46%)
  blocking collectives  63 us (27%)
  starting transfers between devices  21.7 us (9%)
  between operations  14 us (6%)
  matrix products  13.1 us (6%)
  other arithmetic  8.83 us (4%)
  local copies, waits for them, and re-layouts  6.3 us (3%)
    all_gather x1, waiting for transfers between devices, local(): own_whole = lax.all_gather(own_rows, 'sp', axis=1, tiled=True)  53.4 us
    all_gather x1, blocking collectives, local(): piece_key = lax.all_gather(w_key, 'sp', axis=0, tiled=True)  37.8 us
    ppermute x3, waiting for transfers between devices, local(): lax.ppermute(ring[-1], 'sp', [(dev, (dev + 1) % 4) for dev in range(4)])  36 us
    all_gather x1, blocking collectives, local(): piece_value = lax.all_gather(w_value, 'sp', axis=0, tiled=True)  20.3 us
    ppermute x3, starting transfers between devices, local(): lax.ppermute(ring[-1], 'sp', [(dev, (dev + 1) % 4) for dev in range(4)])  9.96 us
    ppermute x2, starting transfers between devices, padded(): lax.ppermute(lax.slice_in_dim(block, block.shape[dim] - width, None, axis...  9.02 us
    reduce_scatter x1, waiting for transfers between devices, local(): lax.psum_scatter(jnp.dot(features, own_whole, preferred_element_type=jnp....  7.01 us
    ppermute x2, waiting for transfers between devices, padded(): lax.ppermute(lax.slice_in_dim(block, 0, width, axis=dim), axis, backward)  6.09 us
  transfers between devices with their start and end apart: 11, of which 6 were waited for; matrix products, arithmetic and copies ran while one was open for 9% of the time, Pallas kernels for 0%

profile of v1, /device:TPU:0, one launch (start us, length us, event | category | flops | bytes accessed | tf_op | source)
XLA Modules:
  0.0 234.7 jit_solution(8461513362667270436)
XLA Ops:
  6.5 0.7 all-gather.4.cloned.1.call-update
  7.3 0.0 all-gather.6.cloned.1.call-start
  7.3 0.7 all-gather.6.cloned.1.call-update
  8.0 0.0 all-gather.8.cloned.1.call-start
  8.1 3.1 %collective-permute-start.2 = (bf16[512,512]{1,0:T(8,128)(2,1)}, bf16[512,512]{1,0:T(8,128)(2,1)S(1)}, u32[]{:S(2)}, u32[]{:S(2)}) collective-permute-start(bf16[512,512]{1,0:T(8,128)(2,1)} %param.16), channel_id=1, source_target_pairs={{0,8},{8,16},{16,24},{24,0},{1,9},{9,17},{17,25},{25,1},{2,10},{10... | collective-permute-start | bytes 1572872 | tf_op jit(solution)/shard_map/ppermute | solution.py:83
  11.2 1.5 fusion.6
  12.7 37.8 %all_gather.15 = bf16[2048,128]{1,0:T(8,128)(2,1)S(1)} all-gather(bf16[512,128]{1,0:T(8,128)(2,1)} %param.17), channel_id=1, replica_groups=mesh['sp'=4,'fs'=4,'tp'=2] {'sp'}, dimensions={0}, use_global_device_ids=true | all-gather | bytes 655360 | tf_op jit(solution)/shard_map/all_gather | solution.py:87
  50.5 20.3 %all_gather.16 = bf16[2048,128]{1,0:T(8,128)(2,1)S(1)} all-gather(bf16[512,128]{1,0:T(8,128)(2,1)} %param.18), channel_id=1, replica_groups=mesh['sp'=4,'fs'=4,'tp'=2] {'sp'}, dimensions={0}, use_global_device_ids=true | all-gather | bytes 655360 | tf_op jit(solution)/shard_map/all_gather | solution.py:88
  70.8 1.9 fusion.13
  72.8 0.2 multiply_cosine_fusion.1
  73.1 3.0 %collective-permute-start = (bf16[128,256]{0,1:T(8,128)(2,1)S(1)}, bf16[128,256]{0,1:T(8,128)(2,1)S(1)}, u32[]{:S(2)}, u32[]{:S(2)}) collective-permute-start(bf16[128,256]{0,1:T(8,128)(2,1)S(1)} %get-tuple-element.21), channel_id=1, source_target_pairs={{0,8},{8,16},{16,24},{1,9},{9,17},{17,25},{2,10},{10,18},{18,26},{... | collective-permute-start | bytes 196616 | tf_op jit(solution)/shard_map/ppermute | solution.py:19
  76.0 1.3 collective-permute-start.1
  77.3 0.1 constant_dynamic-slice_fusion
  77.4 1.0 pad_maximum_fusion
  78.5 0.0 reduce-scatter.2.cloned.1.call-start
  78.6 2.7 %collective-permute-start.3 = (bf16[512,512]{1,0:T(8,128)(2,1)S(1)}, bf16[512,512]{1,0:T(8,128)(2,1)S(1)}, u32[]{:S(2)}, u32[]{:S(2)}) collective-permute-start(bf16[512,512]{1,0:T(8,128)(2,1)S(1)} %collective-permute-done.2), channel_id=1, source_target_pairs={{0,8},{8,16},{16,24},{24,0},{1,9},{9,17},{17,25},{25,1},{2,10},{10... | collective-permute-start | bytes 1572872 | tf_op jit(solution)/shard_map/ppermute | solution.py:83
  81.3 0.7 fusion.82
  82.0 0.3 fusion.26
  82.2 17.0 %collective-permute-done.3 = bf16[512,512]{1,0:T(8,128)(2,1)S(1)} collective-permute-done((bf16[512,512]{1,0:T(8,128)(2,1)S(1)}, bf16[512,512]{1,0:T(8,128)(2,1)S(1)}, u32[]{:S(2)}, u32[]{:S(2)}) %collective-permute-start.3) | collective-permute-done | bytes 524320 | tf_op jit(solution)/shard_map/ppermute | solution.py:83
  99.3 4.2 %collective-permute-start.4 = (bf16[512,512]{1,0:T(8,128)(2,1)S(1)}, bf16[512,512]{1,0:T(8,128)(2,1)S(1)}, u32[]{:S(2)}, u32[]{:S(2)}) collective-permute-start(bf16[512,512]{1,0:T(8,128)(2,1)S(1)} %collective-permute-done.3), channel_id=1, source_target_pairs={{0,8},{8,16},{16,24},{24,0},{1,9},{9,17},{17,25},{25,1},{2,10},{10... | collective-permute-start | bytes 1572872 | tf_op jit(solution)/shard_map/ppermute | solution.py:83
  103.4 1.7 fusion.83
  105.1 1.3 max.18
  106.4 0.9 pad_maximum_fusion.3
  107.4 18.9 %collective-permute-done.4 = bf16[512,512]{1,0:T(8,128)(2,1)S(1)} collective-permute-done((bf16[512,512]{1,0:T(8,128)(2,1)S(1)}, bf16[512,512]{1,0:T(8,128)(2,1)S(1)}, u32[]{:S(2)}, u32[]{:S(2)}) %collective-permute-start.4) | collective-permute-done | bytes 524320 | tf_op jit(solution)/shard_map/ppermute | solution.py:83
  126.7 1.1 fusion.9
  127.8 0.1 subtract_convert_fusion.1
  127.9 0.8 fusion.5
  128.7 0.1 broadcast_maximum_fusion
  128.8 1.9 copy-done
  130.7 0.9 fusion.4
  131.6 0.1 exponential_add_fusion
  131.7 0.0 all-gather.4.cloned.1.call-done
  131.7 3.7 %all-gather.6.cloned.1.call-done = bf16[2048,512]{1,0:T(8,128)(2,1)} async-done(((bf16[512,512]{1,0:T(8,128)(2,1)}), bf16[2048,512]{1,0:T(8,128)(2,1)}) %all-gather.6.cloned.1.call-update) | async-done | bytes 2097168 | tf_op jit(solution)/shard_map/all_gather | solution.py:90
  135.4 3.7 %fusion = f32[256,1024]{1,0:T(8,128)S(1)} fusion(bf16[2048,512]{1,0:T(8,128)(2,1)} %all-gather.6.cloned.1.call-done, bf16[2048,512]{1,0:T(8,128)(2,1)} %all-gather.4.cloned.1.call-done, bf16[256,2048]{1,0:T(8,128)(2,1)S(1)} %copy-done.3, f32[2048]{0:T(1024)S(1)} %copy-done.42, f32[256]{0:T(256)S(1)} %copy-done.40), kind=kOutput, calls=%fused_computation | convolution fusion | flops 1084227584 | bytes 6300672 | tf_op jit(solution)/shard_map/dot_general | solution.py:97
  139.1 0.1 fusion.24
  139.3 6.1 %collective-permute-start.5 = (bf16[15,512]{1,0:T(8,128)(2,1)S(1)}, bf16[15,512]{1,0:T(8,128)(2,1)S(1)}, u32[]{:S(2)}, u32[]{:S(2)}) collective-permute-start(bf16[15,512]{1,0:T(8,128)(2,1)S(1)} %get-tuple-element.15), channel_id=1, source_target_pairs={{0,8},{8,16},{16,24},{1,9},{9,17},{17,25},{2,10},{10,18},{18,26},{... | collective-permute-start | bytes 46088 | tf_op jit(solution)/shard_map/ppermute | solution.py:19
  145.3 1.3 collective-permute-start.6
  146.9 1.2 fusion.12
  148.2 0.1 copy.27
  148.3 6.1 %collective-permute-done.6 = bf16[15,512]{1,0:T(8,128)(2,1)S(1)} collective-permute-done((bf16[15,512]{1,0:T(8,128)(2,1)S(1)}, bf16[15,512]{1,0:T(8,128)(2,1)S(1)}, u32[]{:S(2)}, u32[]{:S(2)}) %collective-permute-start.6) | collective-permute-done | bytes 15392 | tf_op jit(solution)/shard_map/ppermute | solution.py:22
  154.7 3.1 %fusion.79 = (f32[256]{0:T(256)S(1)}, f32[256,512]{1,0:T(8,128)S(1)}) fusion(bf16[15,512]{1,0:T(8,128)(2,1)S(1)} %collective-permute-done.6, bf16[256,512]{1,0:T(8,128)(2,1)S(1)} %fusion.24, f32[512]{0:T(512)S(1)} %bitcast.105, f32[512]{0:T(512)S(1)} %bitcast.106, f32[512]{0:T(512)S(1)} %bitcast.77, f32[512]{0:T(512)S(1)} %bitcast.78, f32[512]{0:T(512)S(1)} %bitcast.79, ...), kind=kLoop, calls=%fused_computation.177 | loop fusion | flops 24116992 | bytes 883712 | tf_op jit(solution)/shard_map/reduce_sum | solution.py:146
  157.8 2.5 %psum.14 = f32[256]{0:T(256)S(1)} all-reduce(f32[256]{0:T(256)S(1)} %get-tuple-element.5), channel_id=1, replica_groups=mesh['sp'=4,'fs'=4,'tp'=2] {'tp'}, use_global_device_ids=true, to_apply=%region_4.5 | all-reduce | flops 256 | bytes 2048 | tf_op jit(solution)/shard_map/psum | solution.py:146
  160.3 0.2 multiply_reduce_fusion
  160.5 2.5 %psum.15 = f32[256]{0:T(256)S(1)} all-reduce(f32[256]{0:T(256)S(1)} %multiply_reduce_fusion), channel_id=1, replica_groups=mesh['sp'=4,'fs'=4,'tp'=2] {'tp'}, use_global_device_ids=true, to_apply=%region_6.7 | all-reduce | flops 256 | bytes 2048 | tf_op jit(solution)/shard_map/psum | solution.py:148
  163.0 0.3 multiply_convert_fusion
  163.2 53.4 %all-gather.8.cloned.1.call-done = bf16[1024,2048]{1,0:T(8,128)(2,1)} async-done(((bf16[1024,512]{1,0:T(8,128)(2,1)}), bf16[1024,2048]{1,0:T(8,128)(2,1)}) %all-gather.8.cloned.1.call-update) | async-done | bytes 4194320 | tf_op jit(solution)/shard_map/all_gather | solution.py:161
  216.6 4.4 %convolution_convert_fusion = bf16[256,2048]{1,0:T(8,128)(2,1)} fusion(bf16[1024,2048]{1,0:T(8,128)(2,1)} %all-gather.8.cloned.1.call-done, bf16[256,512]{1,0:T(8,128)(2,1)S(1)} %multiply_convert_fusion, bf16[256,512]{1,0:T(8,128)(2,1)S(1)} %copy.27), kind=kOutput, calls=%fused_computation.11 | convolution fusion | flops 1075314688 | bytes 5767168 | tf_op jit(solution)/shard_map/dot_general | solution.py:163
  221.1 7.0 %reduce-scatter.2.cloned.1.call-done = bf16[128,2048]{1,0:T(8,128)(2,1)} async-done(((bf16[256,2048]{1,0:T(8,128)(2,1)}), bf16[128,2048]{1,0:T(8,128)(2,1)}) %reduce-scatter.2.cloned.1.call-update) | async-done | bytes 524304 | tf_op jit(solution)/shard_map/reduce_scatter | solution.py:162
  (115 shorter events, 0.7 us)
Async XLA Ops:
  6.5 70.8 %copy-start.5 = (bf16[1024,512]{1,0:T(8,128)(2,1)S(1)}, bf16[1024,512]{1,0:T(8,128)(2,1)}, u32[]{:S(2)}) copy-start(bf16[1024,512]{1,0:T(8,128)(2,1)} %param.26) | copy-start | bytes 3145732
  6.5 70.8 %copy-start.4 = (bf16[1024,512]{1,0:T(8,128)(2,1)S(1)}, bf16[1024,512]{1,0:T(8,128)(2,1)}, u32[]{:S(2)}) copy-start(bf16[1024,512]{1,0:T(8,128)(2,1)} %param.27) | copy-start | bytes 3145732
  6.5 125.2 %all-gather.4.cloned.1.call-start = ((), (), s32[]{:S(2)}) async-start(), calls=%async_computation.1 | async-start | bytes 2621440 | tf_op jit(solution)/shard_map/all_gather | solution.py:89
  7.3 128.2 %all-gather.6.cloned.1.call-start = ((), (), s32[]{:S(2)}) async-start(), calls=%async_computation.2 | async-start | bytes 2621440 | tf_op jit(solution)/shard_map/all_gather | solution.py:90
  8.0 208.6 %all-gather.8.cloned.1.call-start = ((), (), s32[]{:S(2)}) async-start(), calls=%async_computation.3 | async-start | bytes 5242880 | tf_op jit(solution)/shard_map/all_gather | solution.py:161
  8.1 70.5 %collective-permute-start.2 = (bf16[512,512]{1,0:T(8,128)(2,1)}, bf16[512,512]{1,0:T(8,128)(2,1)S(1)}, u32[]{:S(2)}, u32[]{:S(2)}) collective-permute-start(bf16[512,512]{1,0:T(8,128)(2,1)} %param.16), channel_id=1, source_target_pairs={{0,8},{8,16},{16,24},{24,0},{1,9},{9,17},{17,25},{25,1},{2,10},{10... | collective-permute-start | bytes 1572872 | tf_op jit(solution)/shard_map/ppermute | solution.py:83
  72.7 8.6 %copy-start.6 = (f32[31,512]{1,0:T(8,128)S(1)}, f32[31,512]{1,0:T(8,128)}, u32[]{:S(2)}) copy-start(f32[31,512]{1,0:T(8,128)} %param.22) | copy-start | bytes 190468
  73.1 33.4 %collective-permute-start = (bf16[128,256]{0,1:T(8,128)(2,1)S(1)}, bf16[128,256]{0,1:T(8,128)(2,1)S(1)}, u32[]{:S(2)}, u32[]{:S(2)}) collective-permute-start(bf16[128,256]{0,1:T(8,128)(2,1)S(1)} %get-tuple-element.21), channel_id=1, source_target_pairs={{0,8},{8,16},{16,24},{1,9},{9,17},{17,25},{2,10},{10,18},{18,26},{... | collective-permute-start | bytes 196616 | tf_op jit(solution)/shard_map/ppermute | solution.py:19
  76.0 30.4 %collective-permute-start.1 = (bf16[128,256]{0,1:T(8,128)(2,1)S(1)}, bf16[128,256]{0,1:T(8,128)(2,1)}, u32[]{:S(2)}, u32[]{:S(2)}) collective-permute-start(bf16[128,256]{0,1:T(8,128)(2,1)S(1)} %get-tuple-element.22), channel_id=1, source_target_pairs={{8,0},{16,8},{24,16},{9,1},{17,9},{25,17},{10,2},{18,10},{26,18},{... | collective-permute-start | bytes 196616 | tf_op jit(solution)/shard_map/ppermute | solution.py:22
  77.4 49.0 %copy-start.2 = (bf16[512,512]{1,0:T(8,128)(2,1)S(1)}, bf16[512,512]{1,0:T(8,128)(2,1)}, u32[]{:S(2)}) copy-start(bf16[512,512]{1,0:T(8,128)(2,1)} %param.16) | copy-start | bytes 1572868
  78.5 149.6 %reduce-scatter.2.cloned.1.call-start = ((), (), s32[]{:S(2)}) async-start(), calls=%async_computation.4 | async-start | bytes 1572864 | tf_op jit(solution)/shard_map/reduce_scatter | solution.py:162
  78.6 20.7 %collective-permute-start.3 = (bf16[512,512]{1,0:T(8,128)(2,1)S(1)}, bf16[512,512]{1,0:T(8,128)(2,1)S(1)}, u32[]{:S(2)}, u32[]{:S(2)}) collective-permute-start(bf16[512,512]{1,0:T(8,128)(2,1)S(1)} %collective-permute-done.2), channel_id=1, source_target_pairs={{0,8},{8,16},{16,24},{24,0},{1,9},{9,17},{17,25},{25,1},{2,10},{10... | collective-permute-start | bytes 1572872 | tf_op jit(solution)/shard_map/ppermute | solution.py:83
  99.3 27.0 %collective-permute-start.4 = (bf16[512,512]{1,0:T(8,128)(2,1)S(1)}, bf16[512,512]{1,0:T(8,128)(2,1)S(1)}, u32[]{:S(2)}, u32[]{:S(2)}) collective-permute-start(bf16[512,512]{1,0:T(8,128)(2,1)S(1)} %collective-permute-done.3), channel_id=1, source_target_pairs={{0,8},{8,16},{16,24},{24,0},{1,9},{9,17},{17,25},{25,1},{2,10},{10... | collective-permute-start | bytes 1572872 | tf_op jit(solution)/shard_map/ppermute | solution.py:83
  107.3 19.3 %copy-start.3 = (bf16[256,2048]{1,0:T(8,128)(2,1)S(1)}, bf16[256,2048]{1,0:T(8,128)(2,1)}, u32[]{:S(2)}) copy-start(bf16[256,2048]{1,0:T(8,128)(2,1)} %param.14) | copy-start | bytes 3145732
  107.3 19.3 %copy-start.39 = (f32[256]{0:T(256)S(1)}, f32[256]{0:T(256)}, u32[]{:S(2)}) copy-start(f32[256]{0:T(256)} %copy-done.38) | copy-start | bytes 3076
  107.4 19.3 %copy-start.41 = (f32[2048]{0:T(1024)S(1)}, f32[2048]{0:T(1024)}, u32[]{:S(2)}) copy-start(f32[2048]{0:T(1024)} %param.15) | copy-start | bytes 24580
  135.4 11.2 %copy-start.1 = (f32[2,512,256,4]{2,1,3,0:T(8,128)S(1)}, f32[2,512,256,4]{2,1,3,0:T(8,128)}, u32[]{:S(2)}) copy-start(f32[2,512,256,4]{2,1,3,0:T(8,128)} %copy-done) | copy-start | bytes 12582916
  139.3 9.1 %collective-permute-start.5 = (bf16[15,512]{1,0:T(8,128)(2,1)S(1)}, bf16[15,512]{1,0:T(8,128)(2,1)S(1)}, u32[]{:S(2)}, u32[]{:S(2)}) collective-permute-start(bf16[15,512]{1,0:T(8,128)(2,1)S(1)} %get-tuple-element.15), channel_id=1, source_target_pairs={{0,8},{8,16},{16,24},{1,9},{9,17},{17,25},{2,10},{10,18},{18,26},{... | collective-permute-start | bytes 46088 | tf_op jit(solution)/shard_map/ppermute | solution.py:19
  145.3 9.1 %collective-permute-start.6 = (bf16[15,512]{1,0:T(8,128)(2,1)S(1)}, bf16[15,512]{1,0:T(8,128)(2,1)S(1)}, u32[]{:S(2)}, u32[]{:S(2)}) collective-permute-start(bf16[15,512]{1,0:T(8,128)(2,1)S(1)} %get-tuple-element.16), channel_id=1, source_target_pairs={{8,0},{16,8},{24,16},{9,1},{17,9},{25,17},{10,2},{18,10},{26,18},{... | collective-permute-start | bytes 46088 | tf_op jit(solution)/shard_map/ppermute | solution.py:22
  146.6 7.8 %copy-start.7 = (f32[1,512]{1,0:T(1,128)S(1)}, f32[1,512]{1,0:T(1,128)}, u32[]{:S(2)}) copy-start(f32[1,512]{1,0:T(1,128)} %get-tuple-element.29) | copy-start | bytes 6148
  146.6 7.8 %copy-start.8 = (f32[1,512]{1,0:T(1,128)S(1)}, f32[1,512]{1,0:T(1,128)}, u32[]{:S(2)}) copy-start(f32[1,512]{1,0:T(1,128)} %get-tuple-element.30) | copy-start | bytes 6148
  146.6 7.8 %copy-start.9 = (f32[1,512]{1,0:T(1,128)S(1)}, f32[1,512]{1,0:T(1,128)}, u32[]{:S(2)}) copy-start(f32[1,512]{1,0:T(1,128)} %get-tuple-element.31) | copy-start | bytes 6148
  146.7 7.8 %copy-start.10 = (f32[1,512]{1,0:T(1,128)S(1)}, f32[1,512]{1,0:T(1,128)}, u32[]{:S(2)}) copy-start(f32[1,512]{1,0:T(1,128)} %get-tuple-element.32) | copy-start | bytes 6148
  146.7 7.8 %copy-start.11 = (f32[1,512]{1,0:T(1,128)S(1)}, f32[1,512]{1,0:T(1,128)}, u32[]{:S(2)}) copy-start(f32[1,512]{1,0:T(1,128)} %get-tuple-element.33) | copy-start | bytes 6148
  146.7 7.8 %copy-start.12 = (f32[1,512]{1,0:T(1,128)S(1)}, f32[1,512]{1,0:T(1,128)}, u32[]{:S(2)}) copy-start(f32[1,512]{1,0:T(1,128)} %get-tuple-element.34) | copy-start | bytes 6148
  146.7 7.8 %copy-start.13 = (f32[1,512]{1,0:T(1,128)S(1)}, f32[1,512]{1,0:T(1,128)}, u32[]{:S(2)}) copy-start(f32[1,512]{1,0:T(1,128)} %get-tuple-element.35) | copy-start | bytes 6148
  146.7 7.8 %copy-start.14 = (f32[1,512]{1,0:T(1,128)S(1)}, f32[1,512]{1,0:T(1,128)}, u32[]{:S(2)}) copy-start(f32[1,512]{1,0:T(1,128)} %get-tuple-element.36) | copy-start | bytes 6148
  146.7 7.8 %copy-start.15 = (f32[1,512]{1,0:T(1,128)S(1)}, f32[1,512]{1,0:T(1,128)}, u32[]{:S(2)}) copy-start(f32[1,512]{1,0:T(1,128)} %get-tuple-element.37) | copy-start | bytes 6148
  146.7 7.8 %copy-start.16 = (f32[1,512]{1,0:T(1,128)S(1)}, f32[1,512]{1,0:T(1,128)}, u32[]{:S(2)}) copy-start(f32[1,512]{1,0:T(1,128)} %get-tuple-element.38) | copy-start | bytes 6148
  146.7 7.8 %copy-start.17 = (f32[1,512]{1,0:T(1,128)S(1)}, f32[1,512]{1,0:T(1,128)}, u32[]{:S(2)}) copy-start(f32[1,512]{1,0:T(1,128)} %get-tuple-element.39) | copy-start | bytes 6148
  146.7 7.8 %copy-start.18 = (f32[1,512]{1,0:T(1,128)S(1)}, f32[1,512]{1,0:T(1,128)}, u32[]{:S(2)}) copy-start(f32[1,512]{1,0:T(1,128)} %get-tuple-element.40) | copy-start | bytes 6148
  146.7 7.8 %copy-start.19 = (f32[1,512]{1,0:T(1,128)S(1)}, f32[1,512]{1,0:T(1,128)}, u32[]{:S(2)}) copy-start(f32[1,512]{1,0:T(1,128)} %get-tuple-element.41) | copy-start | bytes 6148
  146.8 7.8 %copy-start.20 = (f32[1,512]{1,0:T(1,128)S(1)}, f32[1,512]{1,0:T(1,128)}, u32[]{:S(2)}) copy-start(f32[1,512]{1,0:T(1,128)} %get-tuple-element.42) | copy-start | bytes 6148
  146.8 7.8 %copy-start.21 = (f32[1,512]{1,0:T(1,128)S(1)}, f32[1,512]{1,0:T(1,128)}, u32[]{:S(2)}) copy-start(f32[1,512]{1,0:T(1,128)} %get-tuple-element.43) | copy-start | bytes 6148
  146.8 7.8 %copy-start.22 = (f32[1,512]{1,0:T(1,128)S(1)}, f32[1,512]{1,0:T(1,128)}, u32[]{:S(2)}) copy-start(f32[1,512]{1,0:T(1,128)} %get-tuple-element.44) | copy-start | bytes 6148
  146.8 7.8 %copy-start.23 = (f32[1,512]{1,0:T(1,128)S(1)}, f32[1,512]{1,0:T(1,128)}, u32[]{:S(2)}) copy-start(f32[1,512]{1,0:T(1,128)} %get-tuple-element.45) | copy-start | bytes 6148
  146.8 7.8 %copy-start.24 = (f32[1,512]{1,0:T(1,128)S(1)}, f32[1,512]{1,0:T(1,128)}, u32[]{:S(2)}) copy-start(f32[1,512]{1,0:T(1,128)} %get-tuple-element.46) | copy-start | bytes 6148
  146.8 7.8 %copy-start.25 = (f32[1,512]{1,0:T(1,128)S(1)}, f32[1,512]{1,0:T(1,128)}, u32[]{:S(2)}) copy-start(f32[1,512]{1,0:T(1,128)} %get-tuple-element.47) | copy-start | bytes 6148
  146.8 7.8 %copy-start.26 = (f32[1,512]{1,0:T(1,128)S(1)}, f32[1,512]{1,0:T(1,128)}, u32[]{:S(2)}) copy-start(f32[1,512]{1,0:T(1,128)} %get-tuple-element.48) | copy-start | bytes 6148
  146.8 7.8 %copy-start.27 = (f32[1,512]{1,0:T(1,128)S(1)}, f32[1,512]{1,0:T(1,128)}, u32[]{:S(2)}) copy-start(f32[1,512]{1,0:T(1,128)} %get-tuple-element.49) | copy-start | bytes 6148
  146.8 7.8 %copy-start.28 = (f32[1,512]{1,0:T(1,128)S(1)}, f32[1,512]{1,0:T(1,128)}, u32[]{:S(2)}) copy-start(f32[1,512]{1,0:T(1,128)} %get-tuple-element.50) | copy-start | bytes 6148
  146.8 7.8 %copy-start.29 = (f32[1,512]{1,0:T(1,128)S(1)}, f32[1,512]{1,0:T(1,128)}, u32[]{:S(2)}) copy-start(f32[1,512]{1,0:T(1,128)} %get-tuple-element.51) | copy-start | bytes 6148
  146.9 7.8 %copy-start.30 = (f32[1,512]{1,0:T(1,128)S(1)}, f32[1,512]{1,0:T(1,128)}, u32[]{:S(2)}) copy-start(f32[1,512]{1,0:T(1,128)} %get-tuple-element.52) | copy-start | bytes 6148
  146.9 7.8 %copy-start.31 = (f32[1,512]{1,0:T(1,128)S(1)}, f32[1,512]{1,0:T(1,128)}, u32[]{:S(2)}) copy-start(f32[1,512]{1,0:T(1,128)} %get-tuple-element.53) | copy-start | bytes 6148
  146.9 7.8 %copy-start.32 = (f32[1,512]{1,0:T(1,128)S(1)}, f32[1,512]{1,0:T(1,128)}, u32[]{:S(2)}) copy-start(f32[1,512]{1,0:T(1,128)} %get-tuple-element.54) | copy-start | bytes 6148
  146.9 7.8 %copy-start.33 = (f32[1,512]{1,0:T(1,128)S(1)}, f32[1,512]{1,0:T(1,128)}, u32[]{:S(2)}) copy-start(f32[1,512]{1,0:T(1,128)} %get-tuple-element.55) | copy-start | bytes 6148
  146.9 16.0 %copy-start.36 = (f32[512]{0:T(512)S(1)}, f32[512]{0:T(512)}, u32[]{:S(2)}) copy-start(f32[512]{0:T(512)} %param.25) | copy-start | bytes 6148
  146.9 16.0 %copy-start.37 = (f32[512]{0:T(512)S(1)}, f32[512]{0:T(512)}, u32[]{:S(2)}) copy-start(f32[512]{0:T(512)} %param.24) | copy-start | bytes 6148
  (6 other events, 27.8 us)
Sparse Core Ops, SparseCore 0:
  8.9 68.2 all-gather.3
  78.8 56.6 all-gather.5
  137.0 79.6 all-gather.7
  221.2 6.8 reduce-scatter.1
